TPU v7x, 32 devices: a whole 2x2x4 slice. The times are simulated.
32 devices in a mesh: sp: 8 (over z, core), tp: 4 (over y, x).
Axes of the slice: x: 2, y: 2, z: 4, core: 2. Of those that a mesh axis runs over, the one named last changes fastest.
Arguments:
- residual: bfloat16 [1536, 2048], P('sp'), may hold values from -6 to 6
- query_in: bfloat16 [1536, 2048], P('sp', 'tp'), may hold values from -6 to 6
- value_in: bfloat16 [1536, 2048], P('sp', 'tp'), may hold values from -6 to 6
- forget_fwd: bfloat16 [1536, 2048], P('sp', 'tp'), may hold values from -4.5 to 4.5
- forget_bwd: bfloat16 [1536, 2048], P('sp', 'tp'), may hold values from -4.5 to 4.5
- jumps: float32 [16, 1536], P('tp', 'sp'), may hold values from -2.8 to 0
- gate_gap: float32 [2, 2048], P(None, 'tp'), may hold values from 0 to 0.1
- out_gate: bfloat16 [1536, 2048], P('sp', 'tp'), may hold values from -6 to 6
- head_gain: float32 [2048], P('tp'), may hold values from 0.1 to 1.9
- out_weight: bfloat16 [2048, 2048], P('tp'), may hold values from -0.25 to 0.25
- norm_gain: float32 [2048], replicated, may hold values from 0.1 to 1.9
- route_ids: int32 [1536, 4], P('sp'), may hold values from 0 to 31, all different within a row; in each aligned block of 192 rows (0 to 191, 192 to 383, ...) at most 36 rows name the same one
- route_weights: float32 [1536, 4], P('sp'), may hold values from 0.05 to 0.5
- w_gate: bfloat16 [32, 2048, 4096], P('sp', None, 'tp'), may hold values from -0.375 to 0.375
- w_up: bfloat16 [32, 2048, 4096], P('sp', None, 'tp'), may hold values from -0.375 to 0.375
- w_down: bfloat16 [32, 4096, 2048], P('sp', None, 'tp'), may hold values from -0.09375 to 0.09375
Outputs:
- mixed: bfloat16 [1536, 2048], P('sp', 'tp')
Inputs may be any that keep to these rules, and one draw needn't show every extreme that they name: `route_ids`: in each aligned block of 192 rows each expert is named by at most 36 rows, and by exactly 36 in some block; each row names 4 different experts.
All inputs are finite; a program needn't handle non-finite values.
Results may differ from a plain program's by a relative error of at most 0.024.
Values may be sent and summed in bfloat16 or wider, within the bound.
A program may use at most 128 MiB of HBM per device.

v0:
```python
import math

import jax
import jax.numpy as jnp
from jax import lax
from jax.sharding import PartitionSpec as P

EXPERTS = 32
CAP = 36


highest_precision = lax.Precision.HIGHEST
eps_norm = 1e-06
limit_value = 7.0
alpha_value = 1.702


def entering(x, axis, join, neutral, backward):
    count = lax.axis_size(axis)
    place = lax.axis_index(axis)
    ahead = count - 1 - place if backward else place
    gathered = jax.tree.map(
        lambda a, kind: lax.all_gather(a.astype(kind), axis),
        x,
        jax.tree.map(lambda a: jnp.bfloat16 if a.dtype == jnp.float32 else a.dtype, x),
    )
    state = jax.tree.map(lambda a, e: jnp.zeros_like(a) + jnp.asarray(e, a.dtype), x, neutral)

    def one(hop, state):
        source = count - 1 - hop if backward else hop
        return join(
            state,
            jax.tree.map(
                lambda a, own: lax.dynamic_index_in_dim(a, source, 0, False).astype(own.dtype),
                gathered,
                x,
            ),
        )

    return lax.fori_loop(0, ahead, one, state)


def block_pass(queries, keys_in, values, logs):
    head_rows, head_count, head_width = queries.shape
    block_size = math.gcd(head_rows, 64)
    block_count = head_rows // block_size

    def to_blocks(array):
        return array.reshape(block_count, block_size, head_count, array.shape[-1])

    q_block, k_block, v_block, log_block = (
        to_blocks(queries),
        to_blocks(keys_in),
        to_blocks(values),
        to_blocks(logs),
    )
    decay_sums = jnp.cumsum(log_block, axis=1)
    middle = decay_sums[:, block_size // 2 - 1 : block_size // 2]
    scores = jnp.einsum(
        "nthk,nshk->nhts",
        q_block * jnp.exp(decay_sums - middle),
        k_block * jnp.exp(middle - decay_sums),
        precision=highest_precision,
    )
    lower_mask = jnp.tril(jnp.ones((block_size, block_size), bool))
    within = jnp.einsum(
        "nhts,nshv->nthv", jnp.where(lower_mask, scores, 0.0), v_block, precision=highest_precision
    )
    block_end = decay_sums[:, -1]
    q_start = q_block * jnp.exp(decay_sums)
    k_end = k_block * jnp.exp(block_end[:, None] - decay_sums)

    def advance(current_state, block_items):
        query_segment, key_segment, value_segment, decay_part = block_items
        state_readout = jnp.einsum(
            "qwe,wei->qwi", query_segment, current_state, precision=highest_precision
        )
        current_state = current_state * jnp.exp(decay_part)[:, :, None] + jnp.einsum(
            "foj,fox->ojx", key_segment, value_segment, precision=highest_precision
        )
        return (current_state, state_readout)

    zero_state = jnp.zeros((head_count, head_width, values.shape[-1]), jnp.float32)
    final_state, across = lax.scan(advance, zero_state, (q_start, k_end, v_block, block_end))
    return ((within + across).reshape(head_rows, head_count, -1), final_state)


def combine_states(first_part, second_part):
    return (
        first_part[0] * second_part[0],
        second_part[0][:, :, None] * first_part[1] + second_part[1],
    )


def carried(queries, logs, running_state):
    decayed_state = queries * jnp.exp(jnp.cumsum(logs, axis=0))
    return jnp.einsum("una,nae->une", decayed_state, running_state, precision=highest_precision)


def shards(
    residual,
    query_in,
    value_in,
    forget_fwd,
    forget_bwd,
    jumps,
    gate_gap,
    out_gate,
    head_gain,
    out_weight,
    norm_gain,
    route_ids,
    route_weights,
    w_gate,
    w_up,
    w_down,
):
    head_rows, local_width = query_in.shape
    head_count = jumps.shape[0]
    head_width = local_width // head_count

    def by_head(array):
        return array.astype(jnp.float32).reshape(head_rows, head_count, head_width)

    queries = jax.nn.silu(by_head(query_in))
    values = by_head(value_in)
    jump_rows = jnp.transpose(jumps)[:, :, None]

    def gate_terms(forget_in, gap):
        key_share = gap.reshape(head_count, head_width) * jax.nn.sigmoid(-by_head(forget_in))
        return (key_share, jnp.log1p(-key_share) + jump_rows)

    keys_fwd, logs_fwd = gate_terms(forget_fwd, gate_gap[0])
    keys_bwd, logs_bwd = gate_terms(forget_bwd, gate_gap[1])
    ones_part = jnp.ones((head_count, head_width), jnp.float32)
    zero_part = jnp.zeros((head_count, head_width, head_width), jnp.float32)
    local_fwd, final_fwd = block_pass(queries, keys_fwd, values, logs_fwd)
    summary_fwd = (jnp.exp(jnp.sum(logs_fwd, axis=0)), final_fwd)
    carry_fwd = entering(summary_fwd, "sp", combine_states, (ones_part, zero_part), False)[1]
    flip_queries = jnp.flip(queries, 0)
    flip_logs = jnp.flip(logs_bwd, 0)
    local_bwd, final_bwd = block_pass(
        flip_queries, jnp.flip(keys_bwd, 0), jnp.flip(values, 0), flip_logs
    )
    summary_bwd = (jnp.exp(jnp.sum(logs_bwd, axis=0)), final_bwd)
    carry_bwd = entering(summary_bwd, "sp", combine_states, (ones_part, zero_part), True)[1]
    forward_out = local_fwd + carried(queries, logs_fwd, carry_fwd)
    backward_out = jnp.flip(local_bwd + carried(flip_queries, flip_logs, carry_bwd), 0)
    mixed_heads = forward_out + backward_out
    mean_square = jnp.mean(mixed_heads * mixed_heads, axis=-1, keepdims=True)
    normed = (mixed_heads * lax.rsqrt(mean_square + eps_norm)).reshape(head_rows, local_width)
    gated = (normed * head_gain * jax.nn.silu(out_gate.astype(jnp.float32))).astype(jnp.bfloat16)
    head_terms = jnp.dot(gated, out_weight, preferred_element_type=jnp.float32)
    summed = lax.psum(head_terms.astype(jnp.bfloat16), "tp").astype(jnp.float32)
    stream = (residual.astype(jnp.float32) + summed).astype(jnp.bfloat16)
    stream_f = stream.astype(jnp.float32)
    row_scale = lax.rsqrt(jnp.mean(stream_f * stream_f, axis=-1, keepdims=True) + eps_norm)
    normed_rows = (stream_f * row_scale * norm_gain).astype(jnp.bfloat16)
    top_count = route_ids.shape[1]
    flat_ids = route_ids.reshape(-1)
    one_hot = (flat_ids[:, None] == jnp.arange(EXPERTS, dtype=jnp.int32)[None, :]).astype(jnp.int32)
    slot_rank = jnp.sum((jnp.cumsum(one_hot, axis=0) - 1) * one_hot, axis=1)
    slot_index = flat_ids * CAP + slot_rank
    owner_rows = jnp.arange(head_rows * top_count, dtype=jnp.int32) // top_count
    slot_rows = jnp.full((EXPERTS * CAP,), head_rows, jnp.int32).at[slot_index].set(owner_rows)
    padded_rows = jnp.concatenate(
        [normed_rows, jnp.zeros((1, normed_rows.shape[1]), jnp.bfloat16)], axis=0
    )
    tp_index = lax.axis_index("tp")
    part_width = w_down.shape[2]
    column_rows = lax.dynamic_slice_in_dim(padded_rows, tp_index * part_width, part_width, 1)
    buffer = column_rows[slot_rows].reshape(EXPERTS, CAP, part_width)
    arrived = lax.all_to_all(buffer, "sp", split_axis=0, concat_axis=1, tiled=True)
    piece = lax.all_gather(arrived, "tp", axis=2, tiled=True)
    gate_sum = jnp.einsum("esd,edf->esf", piece, w_gate, preferred_element_type=jnp.float32)
    up_sum = jnp.einsum("esd,edf->esf", piece, w_up, preferred_element_type=jnp.float32)
    gate_sum = jnp.minimum(gate_sum, limit_value)
    up_sum = jnp.clip(up_sum, -limit_value, limit_value)
    active = (gate_sum * jax.nn.sigmoid(alpha_value * gate_sum) * (up_sum + 1.0)).astype(
        jnp.bfloat16
    )
    produced = jnp.einsum(
        "esf,efd->esd",
        lax.all_gather(active, "tp", axis=2, tiled=True),
        w_down,
        preferred_element_type=jnp.float32,
    ).astype(jnp.bfloat16)
    returned = lax.all_to_all(produced, "sp", split_axis=1, concat_axis=0, tiled=True)
    picked = returned.reshape(EXPERTS * CAP, part_width)[slot_index].astype(jnp.float32)
    picked = picked.reshape(head_rows, top_count, part_width)
    moe_out = jnp.sum(picked * route_weights[:, :, None], axis=1)
    own_columns = lax.dynamic_slice_in_dim(stream_f, tp_index * part_width, part_width, 1)
    return (own_columns + moe_out).astype(jnp.bfloat16)


def solution(mesh):
    return jax.shard_map(
        shards,
        mesh=mesh,
        in_specs=(
            P("sp", None),
            P("sp", "tp"),
            P("sp", "tp"),
            P("sp", "tp"),
            P("sp", "tp"),
            P("tp", "sp"),
            P(None, "tp"),
            P("sp", "tp"),
            P("tp"),
            P("tp", None),
            P(),
            P("sp", None),
            P("sp", None),
            P("sp", None, "tp"),
            P("sp", None, "tp"),
            P("sp", None, "tp"),
        ),
        out_specs=P("sp", "tp"),
        check_vma=False,
    )
```

profile of v0, /device:TPU:0, one launch (start us, length us, event | category | flops | bytes accessed | tf_op | source)
XLA Modules:
  0.0 458.2 jit_solution(397519966608035810)
XLA Ops:
  12.4 2.5 log-plus-one_add_fusion
  32.4 2.7 exponential_multiply_fusion.3
  35.9 10.8 %while.55 = (s32[]{:T(128)}, f32[4,128,128]{2,1,0:T(8,128)S(1)}, f32[3,64,4,128]{3,1,2,0:T(8,128)}, f32[3,4,128]{2,1,0:T(4,128)S(1)}, f32[3,64,4,128]{3,2,1,0:T(...) while((s32[]{:T(128)}, f32[4,128,128]{2,1,0:T(8,128)S(1)}, ...), condition=%wide.region_10.11_spmd.clone, body=%wide.region_9.10_spmd.clone.sunk | while | flops 100925440 | bytes 1842288 | solution.py:84
  54.3 10.9 %while.54 = (s32[]{:T(128)}, f32[4,128,128]{2,1,0:T(8,128)S(1)}, f32[3,64,4,128]{3,1,2,0:T(8,128)}, f32[3,4,128]{2,1,0:T(4,128)S(1)}, f32[3,64,4,128]{3,2,1,0:T(...) while((s32[]{:T(128)}, f32[4,128,128]{2,1,0:T(8,128)S(1)}, ...), condition=%wide.region_2.3_spmd.clone, body=%wide.region_1.2_spmd.clone.sunk | while | flops 100925440 | bytes 2103924 | solution.py:84
  73.4 13.7 %all_gather.29 = bf16[8,4,128]{2,1,0:T(4,128)(2,1)S(1)} all-gather(bf16[1,4,128]{2,1,0:T(4,128)(2,1)S(1)} %fusion.59), channel_id=1, replica_groups=mesh['sp'=8,'tp'=4] {'sp'}, dimensions={0}, use_global_device_ids=true | all-gather | bytes 9216 | tf_op jit(solution)/shard_map/all_gather | solution.py:23
  93.3 8.7 %all_gather.26 = bf16[8,4,128]{2,1,0:T(4,128)(2,1)S(1)} all-gather(bf16[1,4,128]{2,1,0:T(4,128)(2,1)S(1)} %fusion.58), channel_id=1, replica_groups=mesh['sp'=8,'tp'=4] {'sp'}, dimensions={0}, use_global_device_ids=true | all-gather | bytes 9216 | tf_op jit(solution)/shard_map/all_gather | solution.py:23
  102.0 3.0 reduce-window.26
  105.6 7.9 %while.53 = (s32[]{:T(128)}, f32[4,128,128]{2,1,0:T(8,128)S(1)}, s32[]{:T(128)}, bf16[8,4,128]{2,1,0:T(4,128)(2,1)S(1)}, bf16[8,4,128,128]{3,2,1,0:T(8,128)(2,1)...) while((s32[]{:T(128)}, f32[4,128,128]{2,1,0:T(8,128)S(1)}, s32[]{:T(128)}, ...), condition=%wide.region_13.14_spmd, body=%wide.region_12.13_spmd.sunk | while | flops 197126 | bytes 660627 | solution.py:40
  115.8 3.6 rev.20
  120.2 2.6 convolution_convert_fusion
  123.6 3.4 scatter_custom_fusion
  127.0 43.9 %all-reduce.5.cloned.1.call-done = bf16[192,2048]{1,0:T(8,128)(2,1)} async-done(((bf16[192,2048]{1,0:T(8,128)(2,1)}), bf16[192,2048]{1,0:T(8,128)(2,1)}) %all-reduce.5.cloned.1.call-update) | async-done | bytes 786448 | tf_op jit(solution)/shard_map/psum | solution.py:154
  170.9 2.7 fusion.18
  174.0 4.2 gather_fusion
  178.5 36.6 %all_to_all.33 = bf16[32,36,512]{2,1,0:T(8,128)(2,1)S(1)} all-to-all(bf16[32,36,512]{2,1,0:T(8,128)(2,1)S(1)} %reshape.243), channel_id=1, replica_groups=mesh['sp'=8,'tp'=4] {'sp'}, dimensions={0} | all-to-all | bytes 2359296 | tf_op jit(solution)/shard_map/all_to_all | solution.py:173
  217.3 54.6 %all-gather.7.cloned.1.call-done = bf16[4,288,2048]{2,1,0:T(8,128)(2,1)} async-done(((bf16[4,288,512]{2,1,0:T(8,128)(2,1)}), bf16[4,288,2048]{2,1,0:T(8,128)(2,1)}) %all-gather.7.cloned.1.call-update) | async-done | bytes 4718608 | tf_op jit(solution)/shard_map/all_gather | solution.py:174
  272.0 10.2 %fusion.64 = f32[4,288,1024]{2,1,0:T(8,128)S(1)} fusion(bf16[4,288,2048]{2,1,0:T(8,128)(2,1)} %all-gather.7.cloned.1.call-done, bf16[4,2048,1024]{2,1,0:T(8,128)(2,1)} %param.38), kind=kOutput, calls=%fused_computation.155 | convolution fusion | flops 4831838208 | bytes 26214400 | tf_op jit(solution)/shard_map/esd,edf->esf/dot_general | solution.py:176
  282.2 14.0 %multiply_convert_fusion = bf16[4,288,1024]{2,1,0:T(8,128)(2,1)} fusion(f32[4,288,1024]{2,1,0:T(8,128)S(1)} %fusion.64, bf16[4,288,2048]{2,1,0:T(8,128)(2,1)S(1)} %copy-done.24, bf16[4,2048,1024]{2,1,0:T(8,128)(2,1)} %param.37), kind=kOutput, calls=%fused_computation.36 | convolution fusion | flops 4843634688 | bytes 28573696 | tf_op jit(solution)/shard_map/esd,edf->esf/dot_general | solution.py:175
  296.2 96.4 %all-gather.9.cloned.1.call-done = bf16[4,288,4096]{2,1,0:T(8,128)(2,1)} async-done(((bf16[4,288,1024]{2,1,0:T(8,128)(2,1)}), bf16[4,288,4096]{2,1,0:T(8,128)(2,1)}) %all-gather.9.cloned.1.call-update) | async-done | bytes 9437200 | tf_op jit(solution)/shard_map/all_gather | solution.py:184
  392.6 12.5 %convolution_convert_fusion.1 = bf16[4,288,512]{2,1,0:T(8,128)(2,1)S(1)} fusion(bf16[4,288,4096]{2,1,0:T(8,128)(2,1)} %all-gather.9.cloned.1.call-done, bf16[4,4096,512]{2,1,0:T(8,128)(2,1)} %param.39), kind=kOutput, calls=%fused_computation.42 | convolution fusion | flops 4832428032 | bytes 27394048 | tf_op jit(solution)/shard_map/esf,efd->esd/dot_general | solution.py:182
  407.0 4.6 %all-to-all-start.1 = ((bf16[4,288,512]{2,0,1:T(4,128)(2,1)}), bf16[4,288,512]{2,0,1:T(4,128)(2,1)S(1)}, u32[]{:S(2)}, u32[]{:S(2)}) async-start(bf16[4,288,512]{2,0,1:T(4,128)(2,1)} %copy.132), calls=%async_computation.1 | async-start | bytes 2359296 | tf_op jit(solution)/shard_map/all_to_all | solution.py:188
  411.7 29.2 %all-to-all-done.1 = bf16[4,288,512]{2,0,1:T(4,128)(2,1)S(1)} async-done(((bf16[4,288,512]{2,0,1:T(4,128)(2,1)}), bf16[4,288,512]{2,0,1:T(4,128)(2,1)S(1)}, u32[]{:S(2)}, u32[]{:S(2)}) %all-to-all-start.1) | async-done | bytes 1179680 | tf_op jit(solution)/shard_map/all_to_all | solution.py:188
  441.5 3.3 gather_fusion.1
  444.8 2.6 reshape.249
  (195 shorter events, 88.9 us)
Async XLA Ops:
  6.5 113.6 %copy-start = (bf16[512,2048]{1,0:T(8,128)(2,1)S(1)}, bf16[512,2048]{1,0:T(8,128)(2,1)}, u32[]{:S(2)}) copy-start(bf16[512,2048]{1,0:T(8,128)(2,1)} %param.33) | copy-start | bytes 6291460
  6.5 99.1 %all-gather.13.cloned.1.call-start = ((), (), s32[]{:S(2)}) async-start(), calls=%async_computation.6 | async-start | bytes 1179648 | tf_op jit(solution)/shard_map/all_gather | solution.py:23
  7.5 7.4 %copy-start.10 = (f32[192,4]{1,0:T(8,128)}, f32[192,4]{1,0:T(8,128)S(1)}, u32[]{:S(2)}) copy-start(f32[192,4]{1,0:T(8,128)S(1)} %copy.135) | copy-start | bytes 9220
  14.9 7.6 %copy-start.4 = (f32[192,4,128]{2,1,0:T(4,128)}, f32[192,4,128]{2,1,0:T(4,128)S(1)}, u32[]{:S(2)}) copy-start(f32[192,4,128]{2,1,0:T(4,128)S(1)} %get-tuple-element.371) | copy-start | bytes 1179652
  14.9 3.7 copy-start.15
  21.6 10.0 %copy-start.2 = (f32[192,4,128]{2,1,0:T(4,128)}, f32[192,4,128]{2,1,0:T(4,128)S(1)}, u32[]{:S(2)}) copy-start(f32[192,4,128]{2,1,0:T(4,128)S(1)} %get-tuple-element.370) | copy-start | bytes 1179652
  24.5 4.3 copy-start.9
  47.4 72.0 %all-gather.11.cloned.1.call-start = ((), (), s32[]{:S(2)}) async-start(), calls=%async_computation.5 | async-start | bytes 1179648 | tf_op jit(solution)/shard_map/all_gather | solution.py:23
  54.3 13.4 %copy-start.5 = (f32[192,4,128]{2,1,0:T(4,128)S(1)}, f32[192,4,128]{2,1,0:T(4,128)}, u32[]{:S(2)}) copy-start(f32[192,4,128]{2,1,0:T(4,128)} %copy-done.4) | copy-start | bytes 1179652
  54.3 14.2 %copy-start.18 = (s32[192,4]{0,1:T(4,128)S(1)}, s32[192,4]{0,1:T(4,128)}, u32[]{:S(2)}) copy-start(s32[192,4]{0,1:T(4,128)} %param.35) | copy-start | bytes 9220
  65.9 105.0 %all-reduce.5.cloned.1.call-start = ((), (), s32[]{:S(2)}) async-start(), calls=%async_computation.2 | async-start | bytes 1572864 | tf_op jit(solution)/shard_map/psum | solution.py:154
  69.3 19.6 %copy-start.13 = (f32[3,64,4,128]{3,1,2,0:T(8,128)S(1)}, f32[3,64,4,128]{3,1,2,0:T(8,128)}, u32[]{:S(2)}) copy-start(f32[3,64,4,128]{3,1,2,0:T(8,128)} %get-tuple-element.212) | copy-start | bytes 1179652
  91.8 10.2 %copy-start.17 = (s32[6,128]{1,0:T(8,128)S(1)}, s32[6,128]{1,0:T(8,128)}, u32[]{:S(2)}) copy-start(s32[6,128]{1,0:T(8,128)} %eq.29) | copy-start | bytes 9220
  91.8 13.2 %copy-start.19 = (s32[192,4]{0,1:T(4,128)S(1)}, s32[192,4]{0,1:T(4,128)}, u32[]{:S(2)}) copy-start(s32[192,4]{0,1:T(4,128)} %param.35) | copy-start | bytes 9220
  92.4 21.2 %copy-start.12 = (f32[3,64,4,128]{3,1,0,2:T(8,128)S(1)}, f32[3,64,4,128]{3,1,0,2:T(8,128)}, u32[]{:S(2)}) copy-start(f32[3,64,4,128]{3,1,0,2:T(8,128)} %copy.118) | copy-start | bytes 1179652
  115.8 3.7 copy-start.11
  120.2 50.7 %copy-start.6 = (bf16[192,2048]{1,0:T(8,128)(2,1)S(1)}, bf16[192,2048]{1,0:T(8,128)(2,1)}, u32[]{:S(2)}) copy-start(bf16[192,2048]{1,0:T(8,128)(2,1)} %param.24) | copy-start | bytes 2359300
  122.8 50.9 %copy-start.21 = (f32[2048]{0:T(1024)S(1)}, f32[2048]{0:T(1024)}, u32[]{:S(2)}) copy-start(f32[2048]{0:T(1024)} %param.34) | copy-start | bytes 24580
  122.8 149.2 %all-gather.7.cloned.1.call-start = ((), (), s32[]{:S(2)}) async-start(), calls=%async_computation.3 | async-start | bytes 5898240 | tf_op jit(solution)/shard_map/all_gather | solution.py:174
  217.1 175.5 %all-gather.9.cloned.1.call-start = ((), (), s32[]{:S(2)}) async-start(), calls=%async_computation.4 | async-start | bytes 11796480 | tf_op jit(solution)/shard_map/all_gather | solution.py:184
  272.0 10.2 %copy-start.24 = (bf16[4,288,2048]{2,1,0:T(8,128)(2,1)S(1)}, bf16[4,288,2048]{2,1,0:T(8,128)(2,1)}, u32[]{:S(2)}) copy-start(bf16[4,288,2048]{2,1,0:T(8,128)(2,1)} %all-gather.7.cloned.1.call-done) | copy-start | bytes 14155780
  405.0 6.5 %copy-start.23 = (f32[192,4]{0,1:T(4,128)S(1)}, f32[192,4]{0,1:T(4,128)}, u32[]{:S(2)}) copy-start(f32[192,4]{0,1:T(4,128)} %param.36) | copy-start | bytes 9220
  407.0 34.0 %all-to-all-start.1 = ((bf16[4,288,512]{2,0,1:T(4,128)(2,1)}), bf16[4,288,512]{2,0,1:T(4,128)(2,1)S(1)}, u32[]{:S(2)}, u32[]{:S(2)}) async-start(bf16[4,288,512]{2,0,1:T(4,128)(2,1)} %copy.132), calls=%async_computation.1 | async-start | bytes 2359296 | tf_op jit(solution)/shard_map/all_to_all | solution.py:188
  441.5 10.1 %copy-start.1 = (bf16[512,2048]{1,0:T(8,128)(2,1)S(1)}, bf16[512,2048]{1,0:T(8,128)(2,1)}, u32[]{:S(2)}) copy-start(bf16[512,2048]{1,0:T(8,128)(2,1)} %param.33) | copy-start | bytes 6291460
  (8 other events, 16.7 us)
Sparse Core Ops, SparseCore 0:
  47.5 24.9 all-gather.12
  74.1 21.7 all-gather.10
  122.9 47.9 all-reduce.4
  217.2 54.7 all-gather.6
  296.3 96.1 all-gather.8
where the time goes:
time: 460 us; the launch traced here: 458 us
  waiting for transfers between devices  224 us (49%)
  matrix products  60.6 us (13%)
  blocking collectives  59 us (13%)
  local copies, waits for them, and re-layouts  58.7 us (13%)
  other arithmetic  36.5 us (8%)
  between operations  13.7 us (3%)
  starting transfers between devices  4.99 us (1%)
    all_gather x1, waiting for transfers between devices, shards(): lax.all_gather(active, 'tp', axis=2, tiled=True)  96.4 us
    all_gather x1, waiting for transfers between devices, shards(): piece = lax.all_gather(arrived, 'tp', axis=2, tiled=True)  54.6 us
    psum x1, waiting for transfers between devices, shards(): summed = lax.psum(head_terms.astype(jnp.bfloat16), 'tp').astype(jnp.float32)  43.9 us
    all_to_all x1, blocking collectives, shards(): lax.all_to_all(buffer, 'sp', split_axis=0, concat_axis=1, tiled=True)  36.6 us
    all_to_all x1, waiting for transfers between devices, shards(): lax.all_to_all(produced, 'sp', split_axis=1, concat_axis=0, tiled=True)  29.2 us
    all_gather x2, blocking collectives, entering(): lax.all_gather(a.astype(kind), axis)  22.4 us
    dot_general x1, matrix products, shards(): jnp.einsum('esd,edf->esf', piece, w_gate, preferred_element_type=jnp.floa...  14 us
    dot_general x1, matrix products, shards(): jnp.einsum('esf,efd->esd', lax.all_gather(active, 'tp', axis=2, tiled=Tru...  12.5 us
  transfers between devices with their start and end apart: 6, of which 4 were waited for; matrix products, arithmetic and copies ran while one was open for 12% of the time, Pallas kernels for 0%

commit v1 on v0

--- a/solution.py
+++ b/solution.py
@@ -1,8 +1,11 @@
+import functools
 import math
 
 import jax
 import jax.numpy as jnp
 from jax import lax
+from jax.experimental import pallas as pl
+from jax.experimental.pallas import tpu as pltpu
 from jax.sharding import PartitionSpec as P
 
 EXPERTS = 32
@@ -193,9 +196,593 @@
     return (own_columns + moe_out).astype(jnp.bfloat16)
 
 
+MESH = pl.DeviceIdType.MESH
+f32 = jnp.float32
+bf16 = jnp.bfloat16
+SLOT_PAD = 48
+
+
+def mm(a, b, dims=((1,), (0,))):
+    return lax.dot_general(a.astype(bf16), b.astype(bf16), (dims, ((), ())), preferred_element_type=f32)
+
+
+def mm_exact(a, b, dims=((1,), (0,))):
+    return lax.dot_general(
+        a.astype(f32), b.astype(f32), (dims, ((), ())), precision=highest_precision, preferred_element_type=f32
+    )
+
+
+def remote(src, dst, send, recv, device):
+    return pltpu.make_async_remote_copy(
+        src_ref=src, dst_ref=dst, send_sem=send, recv_sem=recv, device_id=device, device_id_type=MESH
+    )
+
+
+def greet(devices):
+    barrier = pltpu.get_barrier_semaphore()
+    for device in devices:
+        pl.semaphore_signal(barrier, inc=1, device_id=device, device_id_type=MESH)
+    pl.semaphore_wait(barrier, len(devices))
+
+
+def front_kernel(
+    n_sp,
+    n_tp,
+    ids_ref,
+    query_ref,
+    value_ref,
+    ff_ref,
+    fb_ref,
+    jumps_ref,
+    gap_ref,
+    og_ref,
+    hg_ref,
+    ow_ref,
+    res_ref,
+    ng_ref,
+    xs_ref,
+    stream_ref,
+    dslot_ref,
+    st,
+    dec,
+    rst,
+    rdec,
+    pos,
+    rpos,
+    gated,
+    oacc,
+    qcarry,
+    pb,
+    rpb,
+    sq,
+    rsq,
+    rows,
+    st_send,
+    st_recv,
+    dec_send,
+    dec_recv,
+    pos_send,
+    pos_recv,
+    rs_send,
+    rs_recv,
+    sq_send,
+    sq_recv,
+    ag_send,
+    ag_recv,
+):
+    p = lax.axis_index("sp")
+    t = lax.axis_index("tp")
+    n, width = query_ref.shape
+    heads = jumps_ref.shape[0]
+    hw = width // heads
+    n_exp = EXPERTS // n_sp
+    n_z = n_sp // 2
+    group = xs_ref.shape[1] // (2 * CAP)
+    partner = p + 1 - 2 * lax.rem(p, 2)
+    zpeers = [lax.rem(p + 2 * k, n_sp) for k in range(1, n_z)]
+    zfrom = [lax.rem(p + n_sp - 2 * k, n_sp) for k in range(1, n_z)]
+    speers = [lax.rem(p + k, n_sp) for k in range(1, n_sp)]
+    tpeers = [lax.rem(t + k, n_tp) for k in range(1, n_tp)]
+    tfrom = [lax.rem(t + n_tp - k, n_tp) for k in range(1, n_tp)]
+    greet([(s, t) for s in speers] + [(p, u) for u in tpeers])
+
+    row_i = lax.broadcasted_iota(jnp.int32, (n, n), 0)
+    col_i = lax.broadcasted_iota(jnp.int32, (n, n), 1)
+    lower = (col_i <= row_i).astype(f32)
+    upper = (col_i >= row_i).astype(f32)
+    eye = (col_i == row_i).astype(f32)
+
+    ex_i = lax.broadcasted_iota(jnp.int32, (n, EXPERTS), 1)
+    picks = [(ids_ref[:, j : j + 1] == ex_i).astype(f32) for j in range(ids_ref.shape[1])]
+    named = sum(picks)
+    strict_before = (row_i < col_i).astype(f32)
+    named_t = mm(named, eye, ((0,), (0,)))
+    rank_t = mm(named, strict_before, ((0,), (0,)))
+    place = lax.rem(p, group).astype(f32) * CAP
+    table = jnp.where(named_t > 0.5, rank_t + place, -1.0)
+    pos[...] = jnp.full(pos.shape, -1.0, f32)
+    for d in range(n_sp):
+        pos[d, 0:n_exp, :] = table[d * n_exp : (d + 1) * n_exp, :]
+    rank = mm(col_i < row_i, named)
+    base = ex_i.astype(f32) * SLOT_PAD + rank
+    lane = lax.broadcasted_iota(jnp.int32, dslot_ref.shape, 1)
+    slots = jnp.zeros(dslot_ref.shape, f32)
+    for j, pick in enumerate(picks):
+        slots = jnp.where(lane == j, jnp.sum(pick * base, axis=1, keepdims=True), slots)
+    dslot_ref[...] = slots
+
+    def gates(ref, index):
+        key = gap_ref[index : index + 1, :] * jax.nn.sigmoid(-ref[...].astype(f32))
+        return key, jnp.log1p(-key)
+
+    key_f, log_f = gates(ff_ref, 0)
+    key_b, log_b = gates(fb_ref, 1)
+    sum_f = mm_exact(lower, log_f)
+    sum_b = mm_exact(upper, log_b)
+    jcol_f = mm_exact(lower, jumps_ref[...], ((1,), (1,)))
+    jcol_b = mm_exact(upper, jumps_ref[...], ((1,), (1,)))
+    jrow_f = mm_exact(jumps_ref[...], lower, ((1,), (1,)))
+    jrow_b = mm_exact(jumps_ref[...], upper, ((1,), (1,)))
+    query = query_ref[...].astype(f32)
+    query = query * jax.nn.sigmoid(query)
+    end_f, end_b = sum_f[n - 1 : n, :], sum_b[0:1, :]
+    for h in range(heads):
+        cols = slice(h * hw, (h + 1) * hw)
+        for d, (key, total, end, jcol, jend) in enumerate(
+            (
+                (key_f, sum_f, end_f, jcol_f, n - 1),
+                (key_b, sum_b, end_b, jcol_b, 0),
+            )
+        ):
+            jtot = jcol[jend : jend + 1, h : h + 1]
+            decay = jnp.exp(jnp.minimum(end[:, cols] - total[:, cols] + (jtot - jcol[:, h : h + 1]), 0.0))
+            st[d, h * hw : (h + 1) * hw, :] = mm(
+                value_ref[:, cols], key[:, cols] * decay, ((0,), (0,))
+            ).astype(bf16)
+            dec[d, :, cols] = jnp.broadcast_to(jnp.exp(end[:, cols] + jtot), (dec.shape[1], hw))
+            qcarry[d, :, cols] = (
+                query[:, cols] * jnp.exp(total[:, cols] + jcol[:, h : h + 1])
+            ).astype(bf16)
+
+    pending = []
+
+    def go(copy):
+        copy.start()
+        pending.append(copy)
+
+    st_next = 0
+    for peer in [partner] + zpeers:
+        way = jnp.where(peer > p, 0, 1)
+        go(remote(st.at[way], rst.at[p], st_send.at[st_next], st_recv.at[p], (peer, t)))
+        go(remote(dec.at[way], rdec.at[p], dec_send.at[st_next], dec_recv.at[p], (peer, t)))
+        st_next += 1
+    for i, peer in enumerate(speers):
+        go(remote(pos.at[peer], rpos.at[p], pos_send.at[i], pos_recv.at[p], (peer, t)))
+
+    mid_f, mid_b = sum_f[n // 2 : n // 2 + 1, :], sum_b[n // 2 : n // 2 + 1, :]
+    q_f, k_f = query * jnp.exp(sum_f - mid_f), key_f * jnp.exp(mid_f - sum_f)
+    q_b, k_b = query * jnp.exp(sum_b - mid_b), key_b * jnp.exp(mid_b - sum_b)
+    for h in range(heads):
+        cols = slice(h * hw, (h + 1) * hw)
+        jump_f = jnp.exp(jnp.minimum(jcol_f[:, h : h + 1] - jrow_f[h : h + 1, :], 0.0))
+        jump_b = jnp.exp(jnp.minimum(jcol_b[:, h : h + 1] - jrow_b[h : h + 1, :], 0.0))
+        score = mm(q_f[:, cols], k_f[:, cols], ((1,), (1,))) * (jump_f * lower)
+        score += mm(q_b[:, cols], k_b[:, cols], ((1,), (1,))) * (jump_b * upper)
+        oacc[:, cols] = mm(score, value_ref[:, cols])
+
+    def st_wait(source):
+        remote(st.at[0], rst.at[source], st_send.at[0], st_recv.at[source], (partner, t)).wait_recv()
+        remote(dec.at[0], rdec.at[source], dec_send.at[0], dec_recv.at[source], (partner, t)).wait_recv()
+
+    for source in zfrom:
+        st_wait(source)
+        go(remote(rst.at[source], rst.at[source], st_send.at[st_next], st_recv.at[source], (partner, t)))
+        go(remote(rdec.at[source], rdec.at[source], dec_send.at[st_next], dec_recv.at[source], (partner, t)))
+        st_next += 1
+    st_wait(partner)
+    for source in zfrom:
+        st_wait(source + 1 - 2 * lax.rem(p, 2))
+
+    def carry_from(first, step, count, d):
+        def one(hop, states):
+            source = first + step * hop
+            return tuple(
+                rdec[source, 0:1, h * hw : (h + 1) * hw] * states[h]
+                + rst[source, h * hw : (h + 1) * hw, :].astype(f32)
+                for h in range(heads)
+            )
+
+        states = lax.fori_loop(0, count, one, tuple(jnp.zeros((hw, hw), f32) for h in range(heads)))
+        for h in range(heads):
+            cols = slice(h * hw, (h + 1) * hw)
+            oacc[:, cols] += mm(qcarry[d, :, cols], states[h], ((1,), (1,)))
+
+    carry_from(0, 1, p, 0)
+    carry_from(n_sp - 1, -1, n_sp - 1 - p, 1)
+
+    for h in range(heads):
+        cols = slice(h * hw, (h + 1) * hw)
+        out = oacc[:, cols]
+        scale = lax.rsqrt(jnp.mean(out * out, axis=-1, keepdims=True) + eps_norm)
+        gate = og_ref[:, cols].astype(f32)
+        gated[:, cols] = (out * scale * hg_ref[:, cols] * (gate * jax.nn.sigmoid(gate))).astype(bf16)
+
+    for u in range(n_tp):
+        pb[u] = mm(gated[...], ow_ref[:, u * width : (u + 1) * width]).astype(bf16)
+    for i, peer in enumerate(tpeers):
+        go(remote(pb.at[peer], rpb.at[t], rs_send.at[i], rs_recv.at[t], (p, peer)))
+    own = pl.ds(pl.multiple_of(t * width, 128), width)
+    total = pb[t].astype(f32)
+    for source in tfrom:
+        remote(pb.at[0], rpb.at[source], rs_send.at[0], rs_recv.at[source], (p, tpeers[0])).wait_recv()
+        total = total + rpb[source].astype(f32)
+    stream = (res_ref[:, own].astype(f32) + total).astype(bf16)
+    stream_ref[...] = stream
+    stream = stream.astype(f32)
+    sq[...] = mm_exact(jnp.ones((sq.shape[0], width), f32), stream * stream, ((1,), (1,)))
+    for i, peer in enumerate(tpeers):
+        go(remote(sq, rsq.at[t], sq_send.at[i], sq_recv.at[t], (p, peer)))
+    squares = sq[...]
+    for source in tfrom:
+        remote(sq, rsq.at[source], sq_send.at[0], sq_recv.at[source], (p, tpeers[0])).wait_recv()
+        squares = squares + rsq[source]
+    scale = lax.rsqrt(squares / (width * n_tp) + eps_norm)
+    scale = mm_exact(eye, scale, ((1,), (1,)))[:, 0:1]
+    rows[p, t] = (stream * scale * ng_ref[:, own]).astype(bf16)
+
+    ag_next = 0
+
+    def spread(block, share, device):
+        nonlocal ag_next
+        go(
+            remote(
+                rows.at[block, share],
+                rows.at[block, share],
+                ag_send.at[ag_next],
+                ag_recv.at[block, share],
+                device,
+            )
+        )
+        ag_next += 1
+
+    def arrive(block, share):
+        remote(
+            rows.at[block, share],
+            rows.at[block, share],
+            ag_send.at[0],
+            ag_recv.at[block, share],
+            (partner, t),
+        ).wait_recv()
+
+    for peer in zpeers:
+        spread(p, t, (peer, t))
+    for peer in tpeers:
+        spread(p, t, (p, peer))
+    spread(p, t, (partner, t))
+    for block in zfrom:
+        arrive(block, t)
+        for peer in tpeers:
+            spread(block, t, (p, peer))
+        spread(block, t, (partner, t))
+    for block in [p] + zfrom:
+        for share in tfrom:
+            arrive(block, share)
+            spread(block, share, (partner, t))
+    for source in speers:
+        remote(pos.at[0], rpos.at[source], pos_send.at[0], pos_recv.at[source], (partner, t)).wait_recv()
+    rpos[p] = pos[p]
+    for block in [p] + zfrom:
+        other = block + 1 - 2 * lax.rem(p, 2)
+        arrive(other, t)
+        for share in tfrom:
+            arrive(other, share)
+
+    half = group * CAP
+    slot_i = lax.broadcasted_iota(jnp.int32, (half, n), 0).astype(f32)
+    for e in range(n_exp):
+        for g in range(n_sp // group):
+            hot = [(slot_i == rpos[g * group + b, e : e + 1, :]).astype(bf16) for b in range(group)]
+
+            def one(u, unused, hot=hot, g=g, e=e):
+                part = mm(hot[0], rows[g * group, u])
+                for b in range(1, group):
+                    part = part + mm(hot[b], rows[g * group + b, u])
+                xs_ref[
+                    e, g * half : (g + 1) * half, pl.ds(pl.multiple_of(u * width, 128), width)
+                ] = part.astype(bf16)
+                return unused
+
+            lax.fori_loop(0, n_tp, one, 0)
+    for copy in pending:
+        copy.wait_send()
+
+
+def expert_kernel(
+    n_sp,
+    n_tp,
+    xs_ref,
+    wg_ref,
+    wu_ref,
+    wd_ref,
+    stream_ref,
+    dslot_ref,
+    rw_ref,
+    out_ref,
+    gbuf,
+    ubuf,
+    wd,
+    acts,
+    prod,
+    rprod,
+    wsem,
+    dsem,
+    act_send,
+    act_recv,
+    ret_send,
+    ret_recv,
+):
+    p = lax.axis_index("sp")
+    t = lax.axis_index("tp")
+    n_exp, depth, hidden = wg_ref.shape
+    slots = xs_ref.shape[1]
+    tile = gbuf.shape[2]
+    tiles = hidden // tile
+    xn = t + 1 - 2 * lax.rem(t, 2)
+    yn = lax.rem(t + 2, n_tp)
+    dg = n_tp - 1 - t
+    speers = [lax.rem(p + k, n_sp) for k in range(1, n_sp)]
+    half = slots // 2
+    halves = (pl.ds(0, half), pl.ds(half, half))
+
+    def fetch(step, slot):
+        e, i = step // tiles, lax.rem(step, tiles)
+        cols = pl.ds(pl.multiple_of(i * tile, 128), tile)
+        return (
+            pltpu.make_async_copy(wg_ref.at[e, :, cols], gbuf.at[slot], wsem.at[0, slot]),
+            pltpu.make_async_copy(wu_ref.at[e, :, cols], ubuf.at[slot], wsem.at[1, slot]),
+        )
+
+    for step in range(2):
+        for copy in fetch(step, step):
+            copy.start()
+    down = [pltpu.make_async_copy(wd_ref.at[e], wd.at[e], dsem.at[e]) for e in range(n_exp)]
+    greet([(s, t) for s in speers] + [(p, xn), (p, yn)])
+    prod[...] = jnp.zeros(prod.shape, bf16)
+
+    def act_copy(e, block, part, number, device):
+        ref = acts.at[e, block, halves[part]]
+        return remote(ref, ref, act_send.at[e, number], act_recv.at[e, block, part], (p, device))
+
+    def own_sends(e):
+        return (
+            act_copy(e, t, 0, 0, xn),
+            act_copy(e, t, 1, 1, yn),
+            act_copy(e, t, 1, 2, xn),
+            act_copy(e, t, 0, 3, yn),
+        )
+
+    def expert(e, unused):
+        def part(i, unused):
+            step = e * tiles + i
+            slot = lax.rem(step, 2)
+            for copy in fetch(step, slot):
+                copy.wait()
+            x = xs_ref[e]
+            gate = jnp.dot(x, gbuf[slot], preferred_element_type=f32)
+            up = jnp.dot(x, ubuf[slot], preferred_element_type=f32)
+            gate = jnp.minimum(gate, limit_value)
+            up = jnp.clip(up, -limit_value, limit_value)
+            cols = pl.ds(pl.multiple_of(i * tile, 128), tile)
+            acts[e, t, :, cols] = (gate * jax.nn.sigmoid(alpha_value * gate) * (up + 1.0)).astype(bf16)
+
+            @pl.when(step + 2 < n_exp * tiles)
+            def _():
+                for copy in fetch(step + 2, slot):
+                    copy.start()
+
+            return unused
+
+        lax.fori_loop(0, tiles, part, 0)
+        for copy in own_sends(e):
+            copy.start()
+        return unused
+
+    lax.fori_loop(0, n_exp, expert, 0)
+    for copy in down:
+        copy.start()
+
+    def forward(e, unused):
+        act_copy(e, xn, 0, 0, xn).wait_recv()
+        act_copy(e, xn, 0, 4, yn).start()
+        act_copy(e, yn, 1, 0, xn).wait_recv()
+        act_copy(e, yn, 1, 5, xn).start()
+        return unused
+
+    lax.fori_loop(0, n_exp, forward, 0)
+    for copy in down:
+        copy.wait()
+
+    def ret_copy(e, i, peer):
+        return remote(prod.at[e, peer], rprod.at[p, e], ret_send.at[e, i], ret_recv.at[e, p], (peer, t))
+
+    def lower(e, unused):
+        act_copy(e, xn, 1, 0, xn).wait_recv()
+        act_copy(e, yn, 0, 0, xn).wait_recv()
+        act_copy(e, dg, 0, 0, xn).wait_recv()
+        act_copy(e, dg, 1, 0, xn).wait_recv()
+        total = jnp.dot(acts[e, 0], wd[e, 0:hidden, :], preferred_element_type=f32)
+        for u in range(1, n_tp):
+            total += jnp.dot(acts[e, u], wd[e, u * hidden : (u + 1) * hidden, :], preferred_element_type=f32)
+        for s in range(n_sp):
+            prod[e, s, 0:CAP, :] = total[s * CAP : (s + 1) * CAP, :].astype(bf16)
+        for i, peer in enumerate(speers):
+            ret_copy(e, i, peer).start()
+        rprod[p, e] = prod[e, p]
+        return unused
+
+    lax.fori_loop(0, n_exp, lower, 0)
+
+    tokens, width = stream_ref.shape
+    total = stream_ref[...].astype(f32)
+    lane = lax.broadcasted_iota(jnp.int32, (tokens, n_exp * SLOT_PAD), 1).astype(f32)
+
+    def returns(k, total):
+        source = lax.rem(p + n_sp - k, n_sp)
+
+        @pl.when(k > 0)
+        def _():
+            for e in range(n_exp):
+                remote(
+                    prod.at[e, 0], rprod.at[source, e], ret_send.at[e, 0], ret_recv.at[e, source], (speers[0], t)
+                ).wait_recv()
+
+        first = (source * (n_exp * SLOT_PAD)).astype(f32)
+        mix = jnp.zeros(lane.shape, f32)
+        for j in range(rw_ref.shape[1]):
+            mix += jnp.where(dslot_ref[:, j : j + 1] - first == lane, rw_ref[:, j : j + 1], 0.0)
+        high = mix.astype(bf16)
+        low = (mix - high.astype(f32)).astype(bf16)
+        block = rprod[source].reshape(n_exp * SLOT_PAD, width)
+        return (
+            total
+            + jnp.dot(high, block, preferred_element_type=f32)
+            + jnp.dot(low, block, preferred_element_type=f32)
+        )
+
+    total = lax.fori_loop(0, n_sp, returns, total)
+    out_ref[...] = total.astype(bf16)
+
+    def drain(e, unused):
+        for copy in own_sends(e):
+            copy.wait_send()
+        act_copy(e, xn, 0, 4, yn).wait_send()
+        act_copy(e, yn, 1, 5, xn).wait_send()
+        for i, peer in enumerate(speers):
+            ret_copy(e, i, peer).wait_send()
+        return unused
+
+    lax.fori_loop(0, n_exp, drain, 0)
+
+
+def fused(
+    n_sp,
+    n_tp,
+    residual,
+    query_in,
+    value_in,
+    forget_fwd,
+    forget_bwd,
+    jumps,
+    gate_gap,
+    out_gate,
+    head_gain,
+    out_weight,
+    norm_gain,
+    route_ids,
+    route_weights,
+    w_gate,
+    w_up,
+    w_down,
+):
+    tokens, width = query_in.shape
+    heads = jumps.shape[0]
+    hw = width // heads
+    n_exp, model, hidden = w_gate.shape
+    slots = n_sp * CAP
+    vmem = pl.BlockSpec(memory_space=pltpu.VMEM)
+    dma = pltpu.SemaphoreType.DMA
+    group = n_sp // 2
+    n_ag = (n_sp // 2) * n_tp * 2
+    xs, stream, dslot = pl.pallas_call(
+        functools.partial(front_kernel, n_sp, n_tp),
+        out_shape=(
+            jax.ShapeDtypeStruct((n_exp, slots, model), bf16),
+            jax.ShapeDtypeStruct((tokens, width), bf16),
+            jax.ShapeDtypeStruct((tokens, 128), f32),
+        ),
+        in_specs=[vmem] * 12,
+        out_specs=(vmem, vmem, vmem),
+        scratch_shapes=[
+            pltpu.VMEM((2, heads * hw, hw), bf16),
+            pltpu.VMEM((2, 8, width), f32),
+            pltpu.VMEM((n_sp, heads * hw, hw), bf16),
+            pltpu.VMEM((n_sp, 8, width), f32),
+            pltpu.VMEM((n_sp, 8, tokens), f32),
+            pltpu.VMEM((n_sp, 8, tokens), f32),
+            pltpu.VMEM((tokens, width), bf16),
+            pltpu.VMEM((tokens, width), f32),
+            pltpu.VMEM((2, tokens, width), bf16),
+            pltpu.VMEM((n_tp, tokens, width), bf16),
+            pltpu.VMEM((n_tp, tokens, width), bf16),
+            pltpu.VMEM((8, tokens), f32),
+            pltpu.VMEM((n_tp, 8, tokens), f32),
+            pltpu.VMEM((n_sp, n_tp, tokens, width), bf16),
+            dma((n_sp,)),
+            dma((n_sp,)),
+            dma((n_sp,)),
+            dma((n_sp,)),
+            dma((n_sp,)),
+            dma((n_sp,)),
+            dma((n_tp,)),
+            dma((n_tp,)),
+            dma((n_tp,)),
+            dma((n_tp,)),
+            dma((n_ag,)),
+            dma((n_sp, n_tp)),
+        ],
+        compiler_params=pltpu.CompilerParams(
+            collective_id=0, has_side_effects=True, vmem_limit_bytes=48 * 1024 * 1024
+        ),
+        name="front",
+    )(
+        route_ids,
+        query_in,
+        value_in,
+        forget_fwd,
+        forget_bwd,
+        jumps,
+        gate_gap,
+        out_gate,
+        head_gain.reshape(1, width),
+        out_weight,
+        residual,
+        norm_gain.reshape(1, model),
+    )
+    tile = math.gcd(hidden, 512)
+    anywhere = pl.BlockSpec(memory_space=pl.ANY)
+    return pl.pallas_call(
+        functools.partial(expert_kernel, n_sp, n_tp),
+        out_shape=jax.ShapeDtypeStruct((tokens, width), bf16),
+        in_specs=[vmem, anywhere, anywhere, anywhere, vmem, vmem, vmem],
+        out_specs=vmem,
+        scratch_shapes=[
+            pltpu.VMEM((2, model, tile), bf16),
+            pltpu.VMEM((2, model, tile), bf16),
+            pltpu.VMEM((n_exp, hidden * n_tp, width), bf16),
+            pltpu.VMEM((n_exp, n_tp, slots, hidden), bf16),
+            pltpu.VMEM((n_exp, n_sp, SLOT_PAD, width), bf16),
+            pltpu.VMEM((n_sp, n_exp, SLOT_PAD, width), bf16),
+            dma((2, 2)),
+            dma((n_exp,)),
+            dma((n_exp, 6)),
+            dma((n_exp, n_tp, 2)),
+            dma((n_exp, n_sp)),
+            dma((n_exp, n_sp)),
+        ],
+        compiler_params=pltpu.CompilerParams(
+            collective_id=1, has_side_effects=True, vmem_limit_bytes=60 * 1024 * 1024
+        ),
+        name="experts",
+    )(xs, w_gate, w_up, w_down, stream, dslot, route_weights)
+
+
 def solution(mesh):
+    n_sp, n_tp = mesh.shape["sp"], mesh.shape["tp"]
+    square = n_tp == 4 and n_sp % 2 == 0 and n_sp <= 8
+    program = functools.partial(fused, n_sp, n_tp) if square else shards
+
     return jax.shard_map(
-        shards,
+        program,
         mesh=mesh,
         in_specs=(
             P("sp", None),

time: 460 us -> 216 us (0.47)
  waiting for transfers between devices: 224 us -> 0 us
  Pallas kernels: 0 us -> 200 us
  matrix products: 60.6 us -> 0 us
  blocking collectives: 59 us -> 0 us
  local copies, waits for them, and re-layouts: 58.7 us -> 15.3 us
  other arithmetic: 36.5 us -> 0 us
  between operations: 13.7 us -> 0.05 us
  starting transfers between devices: 4.99 us -> 0 us
    pallas_call x0 -> x2, Pallas kernels: none -> 200 us  [the longest x1 112 us: fused(): pl.pallas_call(functools.partial(expert_kernel, n_sp, n_tp), out_shape=ja...]
    all_gather x4 -> x0, waiting for transfers between devices: 151 us -> none  [the longest x1 96.4 us: shards(): lax.all_gather(active, 'tp', axis=2, tiled=True)]
    dot_general x22 -> x0, matrix products: 60.6 us -> none  [the longest x1 14 us: shards(): jnp.einsum('esd,edf->esf', piece, w_gate, preferred_element_type=jnp.floa...]
    psum x1 -> x0, waiting for transfers between devices: 43.9 us -> none  [shards(): summed = lax.psum(head_terms.astype(jnp.bfloat16), 'tp').astype(jnp.float32)]
    all_to_all x1 -> x0, blocking collectives: 36.6 us -> none  [shards(): lax.all_to_all(buffer, 'sp', split_axis=0, concat_axis=1, tiled=True)]
    all_to_all x1 -> x0, waiting for transfers between devices: 29.2 us -> none  [shards(): lax.all_to_all(produced, 'sp', split_axis=1, concat_axis=0, tiled=True)]
    all_gather x2 -> x0, blocking collectives: 22.4 us -> none  [entering(): lax.all_gather(a.astype(kind), axis)]
    unnamed x54 -> x29, local copies, waits for them, and re-layouts: 1.13 us -> 15.3 us
  transfers between devices with their start and end apart: 6 -> 0, of which waited for: 4 -> 0; matrix products, arithmetic and copies ran while one was open for 12% -> 0% of each run, Pallas kernels for 0% -> 0%
where the time goes in v1:
time: 216 us; the launch traced here: 215 us
  Pallas kernels  200 us (93%)
  local copies, waits for them, and re-layouts  15.3 us (7%)
    pallas_call x1, Pallas kernels, fused(): pl.pallas_call(functools.partial(expert_kernel, n_sp, n_tp), out_shape=ja...  112 us
    pallas_call x1, Pallas kernels, fused(): pl.pallas_call(functools.partial(front_kernel, n_sp, n_tp), out_shape=(ja...  87.6 us
    unnamed x29, local copies, waits for them, and re-layouts  15.3 us

profile of v1, /device:TPU:0, one launch (start us, length us, event | category | flops | bytes accessed | tf_op | source)
XLA Modules:
  0.0 215.1 jit_solution(17885411991287340419)
XLA Ops:
  0.0 0.8 copy.17.ids_ref
  0.8 1.5 copy.18.rw_ref
  2.3 0.0 copy-start
  2.3 1.6 copy-done
  3.8 0.0 copy-start.1
  3.9 1.1 copy-done.1
  5.0 0.0 copy-start.3
  5.0 0.9 copy-done.3
  5.9 0.0 copy-start.4
  5.9 0.9 copy-done.4
  6.8 0.0 copy-start.5
  6.8 0.9 copy-done.5
  7.8 0.9 copy-done.6
  8.7 0.9 copy-done.7
  9.6 0.7 copy-done.9
  10.3 0.7 copy-done.10
  11.0 0.7 copy-done.11
  11.7 0.7 copy-done.12
  12.4 87.6 %front.1 = (bf16[4,288,2048]{2,1,0:T(8,128)(2,1)}, bf16[192,512]{1,0:T(8,128)(2,1)S(1)}, f32[192,128]{1,0:T(8,128)S(1)}) custom-call(s32[192,4]{1,0:T(8,128)S(1)} %copy.17.ids_ref, bf16[192,512]{1,0:T(8,128)(2,1)S(1)} %copy-done.3, bf16[192,512]{1,0:T(8,128)(2,1)S(1)} %copy-done.4, bf16[192,512]{1,0:T(8,128)(2,1)S(1)} %copy-done.5, ...), custom_call_target="tpu_custom_call" | custom-call | tf_op jit(solution)/shard_map/front/pallas_call | solution.py:696
  100.0 0.0 copy-start.2
  100.0 0.7 copy-done.2
  100.7 0.6 copy-done.8
  101.3 112.2 %experts.1 = bf16[192,512]{1,0:T(8,128)(2,1)} custom-call(bf16[4,288,2048]{2,1,0:T(8,128)(2,1)} %get-tuple-element.8.xs_ref, bf16[4,2048,1024]{2,1,0:T(8,128)(2,1)} %wg_ref.1, bf16[4,2048,1024]{2,1,0:T(8,128)(2,1)} %wu_ref.1, bf16[4,4096,512]{2,1,0:T(8,128)(2,1)} %wd_ref.1, bf16[192,512]{1,0:T(8,128)(2,1)} %copy-done.2, f32[192,128]{1,0:T(8,128)} %copy-done.8, ...), custom_call_target="tpu_custom_call" | custom-call | tf_op jit(solution)/shard_map/experts/pallas_call | solution.py:753
  213.5 1.6 copy.20
  (7 shorter events, 0.0 us)
Async XLA Ops:
  2.3 1.6 copy-start
  3.8 1.1 copy-start.1
  5.0 0.9 copy-start.3
  5.9 0.9 copy-start.4
  6.8 0.9 copy-start.5
  7.8 0.9 copy-start.6
  8.7 0.9 copy-start.7
  9.6 0.7 copy-start.9
  10.3 0.7 copy-start.10
  11.0 0.7 copy-start.11
  11.7 0.7 copy-start.12
  100.0 0.7 copy-start.2
  100.7 0.6 copy-start.8

commit v2 on v1

--- a/solution.py
+++ b/solution.py
@@ -229,6 +229,20 @@
     n_sp,
     n_tp,
     ids_ref,
+    query_in,
+    value_in,
+    ff_in,
+    fb_in,
+    jumps_in,
+    gap_in,
+    og_in,
+    hg_in,
+    ow_in,
+    res_in,
+    ng_in,
+    xs_ref,
+    stream_ref,
+    dslot_ref,
     query_ref,
     value_ref,
     ff_ref,
@@ -240,9 +254,7 @@
     ow_ref,
     res_ref,
     ng_ref,
-    xs_ref,
-    stream_ref,
-    dslot_ref,
+    in_sem,
     st,
     dec,
     rst,
@@ -272,6 +284,26 @@
 ):
     p = lax.axis_index("sp")
     t = lax.axis_index("tp")
+    staged = [
+        pltpu.make_async_copy(source, target, in_sem.at[i])
+        for i, (source, target) in enumerate(
+            (
+                (ff_in, ff_ref),
+                (fb_in, fb_ref),
+                (gap_in, gap_ref),
+                (jumps_in, jumps_ref),
+                (query_in, query_ref),
+                (value_in, value_ref),
+                (og_in, og_ref),
+                (hg_in, hg_ref),
+                (res_in, res_ref),
+                (ng_in, ng_ref),
+                (ow_in, ow_ref),
+            )
+        )
+    ]
+    for copy in staged:
+        copy.start()
     n, width = query_ref.shape
     heads = jumps_ref.shape[0]
     hw = width // heads
@@ -310,6 +342,9 @@
     for j, pick in enumerate(picks):
         slots = jnp.where(lane == j, jnp.sum(pick * base, axis=1, keepdims=True), slots)
     dslot_ref[...] = slots
+
+    for copy in staged[:6]:
+        copy.wait()
 
     def gates(ref, index):
         key = gap_ref[index : index + 1, :] * jax.nn.sigmoid(-ref[...].astype(f32))
@@ -397,6 +432,8 @@
             cols = slice(h * hw, (h + 1) * hw)
             oacc[:, cols] += mm(qcarry[d, :, cols], states[h], ((1,), (1,)))
 
+    for copy in staged[6:]:
+        copy.wait()
     carry_from(0, 1, p, 0)
     carry_from(n_sp - 1, -1, n_sp - 1 - p, 1)
 
@@ -431,50 +468,61 @@
     rows[p, t] = (stream * scale * ng_ref[:, own]).astype(bf16)
 
     ag_next = 0
-
-    def spread(block, share, device):
+    xn = t + 1 - 2 * lax.rem(t, 2)
+    yn = lax.rem(t + 2, n_tp)
+    dg = n_tp - 1 - t
+    cut = n // 2
+
+    def view(block, share, part):
+        ref = rows.at[block, share]
+        return ref if part is None else ref.at[pl.ds(part * cut, cut)]
+
+    def spread(block, share, part, device):
         nonlocal ag_next
-        go(
-            remote(
-                rows.at[block, share],
-                rows.at[block, share],
-                ag_send.at[ag_next],
-                ag_recv.at[block, share],
-                device,
-            )
-        )
+        ref = view(block, share, part)
+        go(remote(ref, ref, ag_send.at[ag_next], ag_recv.at[block, share, part or 0], device))
         ag_next += 1
 
-    def arrive(block, share):
-        remote(
-            rows.at[block, share],
-            rows.at[block, share],
-            ag_send.at[0],
-            ag_recv.at[block, share],
-            (partner, t),
-        ).wait_recv()
+    def arrive(block, share, part=None):
+        ref = view(block, share, part)
+        remote(ref, ref, ag_send.at[0], ag_recv.at[block, share, part or 0], (partner, t)).wait_recv()
+
+    def across(block):
+        spread(block, t, 0, (p, xn))
+        spread(block, t, 1, (p, yn))
+        spread(block, t, 1, (p, xn))
+        spread(block, t, 0, (p, yn))
+        spread(block, t, None, (partner, t))
+
+    def relay(block):
+        arrive(block, xn, 0)
+        spread(block, xn, 0, (p, yn))
+        arrive(block, yn, 1)
+        spread(block, yn, 1, (p, xn))
 
     for peer in zpeers:
-        spread(p, t, (peer, t))
-    for peer in tpeers:
-        spread(p, t, (p, peer))
-    spread(p, t, (partner, t))
+        spread(p, t, None, (peer, t))
+    across(p)
     for block in zfrom:
         arrive(block, t)
-        for peer in tpeers:
-            spread(block, t, (p, peer))
-        spread(block, t, (partner, t))
+        across(block)
     for block in [p] + zfrom:
-        for share in tfrom:
-            arrive(block, share)
-            spread(block, share, (partner, t))
+        relay(block)
+    for block in [p] + zfrom:
+        arrive(block, xn, 1)
+        spread(block, xn, None, (partner, t))
+        arrive(block, yn, 0)
+        spread(block, yn, None, (partner, t))
+        arrive(block, dg, 0)
+        arrive(block, dg, 1)
+        spread(block, dg, None, (partner, t))
     for source in speers:
         remote(pos.at[0], rpos.at[source], pos_send.at[0], pos_recv.at[source], (partner, t)).wait_recv()
     rpos[p] = pos[p]
     for block in [p] + zfrom:
         other = block + 1 - 2 * lax.rem(p, 2)
         arrive(other, t)
-        for share in tfrom:
+        for share in (xn, yn, dg):
             arrive(other, share)
 
     half = group * CAP
@@ -692,7 +740,7 @@
     vmem = pl.BlockSpec(memory_space=pltpu.VMEM)
     dma = pltpu.SemaphoreType.DMA
     group = n_sp // 2
-    n_ag = (n_sp // 2) * n_tp * 2
+    n_ag = (n_sp // 2) * n_tp * 3
     xs, stream, dslot = pl.pallas_call(
         functools.partial(front_kernel, n_sp, n_tp),
         out_shape=(
@@ -700,9 +748,21 @@
             jax.ShapeDtypeStruct((tokens, width), bf16),
             jax.ShapeDtypeStruct((tokens, 128), f32),
         ),
-        in_specs=[vmem] * 12,
+        in_specs=[vmem] + [pl.BlockSpec(memory_space=pl.ANY)] * 11,
         out_specs=(vmem, vmem, vmem),
         scratch_shapes=[
+            pltpu.VMEM((tokens, width), bf16),
+            pltpu.VMEM((tokens, width), bf16),
+            pltpu.VMEM((tokens, width), bf16),
+            pltpu.VMEM((tokens, width), bf16),
+            pltpu.VMEM(jumps.shape, f32),
+            pltpu.VMEM(gate_gap.shape, f32),
+            pltpu.VMEM((tokens, width), bf16),
+            pltpu.VMEM((1, width), f32),
+            pltpu.VMEM(out_weight.shape, bf16),
+            pltpu.VMEM((tokens, model), bf16),
+            pltpu.VMEM((1, model), f32),
+            dma((11,)),
             pltpu.VMEM((2, heads * hw, hw), bf16),
             pltpu.VMEM((2, 8, width), f32),
             pltpu.VMEM((n_sp, heads * hw, hw), bf16),
@@ -728,10 +788,10 @@
             dma((n_tp,)),
             dma((n_tp,)),
             dma((n_ag,)),
-            dma((n_sp, n_tp)),
+            dma((n_sp, n_tp, 2)),
         ],
         compiler_params=pltpu.CompilerParams(
-            collective_id=0, has_side_effects=True, vmem_limit_bytes=48 * 1024 * 1024
+            collective_id=0, has_side_effects=True, vmem_limit_bytes=60 * 1024 * 1024
         ),
         name="front",
     )(

time: 216 us -> 203 us (0.940)
  local copies, waits for them, and re-layouts: 15.3 us -> 4.54 us
    unnamed x29 -> x3, local copies, waits for them, and re-layouts: 15.3 us -> 4.54 us
    pallas_call x1, Pallas kernels: 87.6 us -> 84.8 us  [fused(): pl.pallas_call(functools.partial(front_kernel, n_sp, n_tp), out_shape=(ja...]
where the time goes in v2:
time: 203 us
  Pallas kernels  198 us (98%)
  local copies, waits for them, and re-layouts  4.54 us (2%)
    pallas_call x1, Pallas kernels, fused(): pl.pallas_call(functools.partial(expert_kernel, n_sp, n_tp), out_shape=ja...  114 us
    pallas_call x1, Pallas kernels, fused(): pl.pallas_call(functools.partial(front_kernel, n_sp, n_tp), out_shape=(ja...  84.8 us
    unnamed x3, local copies, waits for them, and re-layouts  4.54 us

profile of v2, /device:TPU:0, one launch (start us, length us, event | category | flops | bytes accessed | tf_op | source)
XLA Modules:
  0.0 202.9 jit_solution(10604663062528454104)
XLA Ops:
  0.0 1.4 copy.17.ids_ref
  1.4 1.5 copy.18.rw_ref
  2.9 84.8 %front.1 = (bf16[4,288,2048]{2,1,0:T(8,128)(2,1)}, bf16[192,512]{1,0:T(8,128)(2,1)}, f32[192,128]{1,0:T(8,128)}) custom-call(s32[192,4]{1,0:T(8,128)} %copy.17.ids_ref, bf16[192,512]{1,0:T(8,128)(2,1)} %query_in.1, bf16[192,512]{1,0:T(8,128)(2,1)} %value_in.1, bf16[192,512]{1,0:T(8,128)(2,1)} %ff_in.1, bf16[192,512]{1,0:T(8,128)(2,1)} %fb_in.1, ...), custom_call_target="tpu_custom_call" | custom-call | tf_op jit(solution)/shard_map/front/pallas_call | solution.py:744
  87.8 113.5 %experts.1 = bf16[192,512]{1,0:T(8,128)(2,1)} custom-call(bf16[4,288,2048]{2,1,0:T(8,128)(2,1)} %get-tuple-element.8.xs_ref, bf16[4,2048,1024]{2,1,0:T(8,128)(2,1)} %wg_ref.1, bf16[4,2048,1024]{2,1,0:T(8,128)(2,1)} %wu_ref.1, bf16[4,4096,512]{2,1,0:T(8,128)(2,1)} %wd_ref.1, bf16[192,512]{1,0:T(8,128)(2,1)} %get-tuple-element.9.stream_ref, ...), custom_call_target="tpu_custom_call" | custom-call | tf_op jit(solution)/shard_map/experts/pallas_call | solution.py:813
  201.3 1.6 copy.20
